TPU v7x, 32 devices: a whole 2x2x4 slice. The times are simulated.
32 devices in a mesh: grp: 2 (over y), sp: 4 (over z), tp: 4 (over x, core).
Axes of the slice: x: 2, y: 2, z: 4, core: 2. Of those that a mesh axis runs over, the one named last changes fastest.
Arguments:
- queries: bfloat16 [4096, 2048], P(('grp', 'sp'), 'tp'), parts along dimension 0, may hold values from -64 to 64
- key_heads: bfloat16 [4096, 4, 64], P(('grp', 'sp'), 'tp'), parts along dimension 0, may hold values from -64 to 64
- value_heads: bfloat16 [4096, 4, 64], P(('grp', 'sp'), 'tp'), parts along dimension 0, may hold values from -6 to 6
- sink_logit: float32 [32], P('tp'), may hold values from 3 to 6
- out_weight: bfloat16 [2048, 2048], P('tp'), may hold values from -0.75 to 0.75
- residual: bfloat16 [4096, 2048], P(('grp', 'sp', 'tp')), parts along dimension 0, may hold values from -6 to 6
- norm_gain: float32 [2048], replicated, may hold values from 0.1 to 1.9
- expert_ids: int32 [4096, 2], P(('grp', 'sp', 'tp')), parts along dimension 0, may hold values from 0 to 15, all different within a row; in each aligned block of 128 rows (0 to 127, 128 to 255, ...) at most 32 rows name the same one
- route_weights: float32 [4096, 2], P(('grp', 'sp', 'tp')), parts along dimension 0, may hold values from 0.1 to 1
- gate_weight: bfloat16 [16, 2048, 512], P(('sp', 'tp')), may hold values from -0.125 to 0.125
- up_weight: bfloat16 [16, 2048, 512], P(('sp', 'tp')), may hold values from -0.125 to 0.125
- down_weight: bfloat16 [16, 512, 2048], P(('sp', 'tp')), may hold values from -0.5 to 0.5
Outputs:
- mixed: bfloat16 [4096, 2048], P(('grp', 'sp', 'tp')), parts along dimension 0
There are 2 independent parts, one for each index of `grp`. A program takes and returns all parts, laid end to end along the dimension named above; an argument that names none is the same for every part. Nothing has to cross between parts.
Inputs may be any that keep to these rules, and one draw needn't show every extreme that they name: `expert_ids`: each row names 2 different experts. In the rows of one device (aligned blocks of 128 rows) no expert is named more than 32 times, and in some blocks one expert is named exactly 32 times.
All inputs are finite; a program needn't handle non-finite values.
Results may differ from a plain program's by a relative error of at most 0.014.
Values may be sent and summed in bfloat16 or wider, within the bound.
A program may use at most 64 MiB of HBM per device.

v0:
```python
import jax
import jax.numpy as jnp
from jax import lax
from jax.sharding import PartitionSpec as P

WINDOW = 128


EPS = 1e-06


def from_behind(value, axis, steps):
    count = lax.axis_size(axis)
    initial, last = (max(0, -steps), min(count, count - steps))
    return lax.ppermute(value, axis, [(source, source + steps) for source in range(initial, last)])


def on_device(
    queries,
    key_heads,
    value_heads,
    sink_logit,
    out_weight,
    residual,
    norm_gain,
    expert_ids,
    route_weights,
    gate_weight,
    up_weight,
    down_weight,
):
    rows_sp = queries.shape[0]
    kv_local = key_heads.shape[1]
    head_dim = key_heads.shape[2]
    heads_local = queries.shape[1] // head_dim
    group_size = heads_local // kv_local
    window = WINDOW
    count_of_blocks = rows_sp // window
    edge = jnp.stack([key_heads[rows_sp - window :], value_heads[rows_sp - window :]])
    tail_rows = from_behind(edge, "sp", 1)
    key_blocks = jnp.concatenate([tail_rows[0], key_heads], 0).reshape(
        count_of_blocks + 1, window, kv_local, head_dim
    )
    value_blocks = jnp.concatenate([tail_rows[1], value_heads], 0).reshape(
        count_of_blocks + 1, window, kv_local, head_dim
    )
    key_span = jnp.concatenate([key_blocks[:-1], key_blocks[1:]], 1)
    value_span = jnp.concatenate([value_blocks[:-1], value_blocks[1:]], 1)
    query_pos = jnp.arange(window, dtype=jnp.int32)[:, None]
    key_pos = jnp.arange(2 * window, dtype=jnp.int32)[None, :]
    distance = query_pos + window - key_pos
    band = (distance >= 0) & (distance < window)
    key_start = (
        lax.axis_index("sp") * rows_sp
        + jnp.arange(count_of_blocks, dtype=jnp.int32)[:, None] * window
        - window
        + key_pos
    )
    allowed = band[None, :, :] & (key_start >= 0)[:, None, :]
    query_blocks = queries.reshape(count_of_blocks, window, kv_local, group_size, head_dim)
    logit_scores = jnp.einsum(
        "bqhgd,bkhd->bhgqk", query_blocks, key_span, preferred_element_type=jnp.float32
    ) * head_dim ** (-0.5)
    logit_scores = jnp.where(allowed[:, None, None], logit_scores, -jnp.inf)
    sink_col = sink_logit.reshape(kv_local, group_size)[None, :, :, None, None]
    row_max = jnp.maximum(jnp.max(logit_scores, axis=-1, keepdims=True), sink_col)
    expd = jnp.exp(logit_scores - row_max)
    row_total = jnp.sum(expd, axis=-1, keepdims=True) + jnp.exp(sink_col - row_max)
    attention_probabilities = (expd / row_total).astype(jnp.bfloat16)
    attended = jnp.einsum(
        "bhgqk,bkhd->bqhgd", attention_probabilities, value_span, preferred_element_type=jnp.float32
    ).astype(jnp.bfloat16)
    attended = attended.reshape(rows_sp, heads_local * head_dim)
    rows_dev = residual.shape[0]
    width = residual.shape[1]
    projected = lax.psum_scatter(
        jnp.dot(attended, out_weight, preferred_element_type=jnp.float32),
        "tp",
        scatter_dimension=0,
        tiled=True,
    )
    stream = (residual.astype(jnp.float32) + projected).astype(jnp.bfloat16)
    wide = stream.astype(jnp.float32)
    normed = (
        wide * lax.rsqrt(jnp.mean(wide * wide, axis=-1, keepdims=True) + EPS) * norm_gain
    ).astype(jnp.bfloat16)
    sp_count = lax.axis_size("sp")
    tp_count = lax.axis_size("tp")
    experts_total = sp_count * tp_count
    top_k = expert_ids.shape[1]
    capacity = max(2, 2 * top_k * rows_dev // experts_total)
    flat_ids = expert_ids.reshape(-1)
    pairs = flat_ids.shape[0]
    onehot = (flat_ids[:, None] == jnp.arange(experts_total, dtype=jnp.int32)[None, :]).astype(
        jnp.int32
    )
    earlier = jnp.cumsum(onehot, axis=0) - onehot
    slot_rank = jnp.sum(earlier * onehot, axis=1)
    flat_slot = flat_ids * capacity + slot_rank
    owner_row = jnp.arange(pairs, dtype=jnp.int32) // top_k
    token_in_slot = jnp.zeros((experts_total * capacity,), jnp.int32).at[flat_slot].set(owner_row)
    filled = jnp.zeros((experts_total * capacity,), jnp.bool_).at[flat_slot].set(True)
    outbox = jnp.where(filled[:, None], normed[token_in_slot], jnp.zeros((), jnp.bfloat16))
    outbox = outbox.reshape(experts_total, capacity, width)
    w_gate_own = gate_weight[0]
    w_up_own = up_weight[0]
    w_down_own = down_weight[0]
    arrived = lax.all_to_all(outbox, ("sp", "tp"), split_axis=0, concat_axis=0, tiled=True)
    rows = arrived.reshape(-1, width)
    gate = jnp.dot(rows, w_gate_own, preferred_element_type=jnp.float32)
    upward = jnp.dot(rows, w_up_own, preferred_element_type=jnp.float32)
    expert_hidden = (jax.nn.silu(gate) * upward).astype(jnp.bfloat16)
    expert_rows = jnp.dot(expert_hidden, w_down_own, preferred_element_type=jnp.float32).astype(
        jnp.bfloat16
    )
    results = expert_rows.reshape(arrived.shape)
    returned = lax.all_to_all(results, ("sp", "tp"), split_axis=0, concat_axis=0, tiled=True)
    picked_rows = returned.reshape(experts_total * capacity, width)[flat_slot].reshape(
        rows_dev, top_k, width
    )
    shares = route_weights / jnp.sum(route_weights, axis=-1, keepdims=True)
    combined = jnp.sum(shares[:, :, None] * picked_rows.astype(jnp.float32), axis=1)
    return (wide + combined).astype(jnp.bfloat16)


def solution(mesh):
    return jax.shard_map(
        on_device,
        mesh=mesh,
        in_specs=(
            P(("grp", "sp"), "tp"),
            P(("grp", "sp"), "tp", None),
            P(("grp", "sp"), "tp", None),
            P("tp"),
            P("tp", None),
            P(("grp", "sp", "tp"), None),
            P(),
            P(("grp", "sp", "tp"), None),
            P(("grp", "sp", "tp"), None),
            P(("sp", "tp"), None, None),
            P(("sp", "tp"), None, None),
            P(("sp", "tp"), None, None),
        ),
        out_specs=P(("grp", "sp", "tp"), None),
        check_vma=False,
    )
```

profile of v0, /device:TPU:31, one launch (start us, length us, event | category | flops | bytes accessed | tf_op | source)
XLA Modules:
  0.0 209.1 jit_solution(1902571107196578965)
XLA Ops:
  6.5 0.0 copy-start
  6.5 0.9 slice_bitcast_fusion.2
  7.5 1.3 collective-permute-start
  8.8 0.9 copy_bitcast_fusion
  9.7 0.1 add_compare_fusion
  9.8 0.2 broadcast_and_fusion
  10.0 0.9 copy_bitcast_fusion.2
  10.8 1.6 reshape.235
  12.5 0.0 collective-permute-done
  12.5 0.0 copy-start.8
  12.5 0.9 fusion.1
  13.4 0.1 broadcast_maximum_fusion
  13.5 0.9 fusion
  14.4 0.1 exponential_add_fusion
  14.5 1.2 fusion.19
  15.7 0.4 copy.23
  16.2 3.2 %fusion.30 = f32[512,2048]{1,0:T(8,128)} fusion(bf16[512,2048]{1,0:T(8,128)(2,1)S(1)} %copy-done, bf16[64,8,4,128]{3,2,1,0:T(4,128)(2,1)S(1)} %bitcast.124), kind=kOutput, calls=%fused_computation.34 | convolution fusion | flops 1073741824 | bytes 6815744 | tf_op jit(solution)/shard_map/dot_general | solution.py:77
  19.4 0.0 reduce-scatter.2.cloned.1.call-update
  19.4 0.7 copy-done.6
  20.1 0.1 copy.26
  20.2 0.1 eq.29
  20.3 0.1 eq.25
  20.5 0.6 reduce-window.6
  21.1 0.2 slice_reduce_fusion
  21.3 0.1 copy.25
  21.4 0.1 mul.85
  21.6 0.1 fusion.45
  21.7 1.4 scatter_custom_fusion.1
  23.1 1.5 scatter_custom_fusion
  24.6 0.1 broadcast_in_dim.56
  24.7 40.5 %reduce-scatter.2.cloned.1.call-done = f32[128,2048]{1,0:T(8,128)} async-done(((f32[512,2048]{1,0:T(8,128)}), f32[128,2048]{1,0:T(8,128)}) %reduce-scatter.2.cloned.1.call-update) | async-done | bytes 1048592 | tf_op jit(solution)/shard_map/reduce_scatter | solution.py:76
  65.1 1.5 fusion.22
  66.6 0.0 copy-done.5
  66.6 0.2 fusion.24
  66.8 3.3 %gather_fusion = bf16[512,2048]{1,0:T(8,128)(2,1)} fusion(bf16[128,2048]{1,0:T(8,128)(2,1)S(1)} %fusion.24, s32[1024]{0:T(1024)S(1)} %pad_clamp_fusion.1), kind=kCustom, calls=%fused_computation | custom fusion | bytes 4196352 | tf_op jit(solution)/shard_map/gather | solution.py:103
  70.2 1.8 broadcast_select_fusion
  72.0 0.0 copy-start.9
  72.0 53.0 %all_to_all.10 = bf16[16,32,2048]{2,1,0:T(8,128)(2,1)S(1)} all-to-all(bf16[16,32,2048]{2,1,0:T(8,128)(2,1)S(1)} %broadcast_select_fusion), channel_id=1, replica_groups=mesh['grp'=2,'sp'=4,'tp'=4] {'sp','tp'}, dimensions={0} | all-to-all | bytes 4194304 | tf_op jit(solution)/shard_map/all_to_all | solution.py:108
  125.0 1.3 copy-done.1
  126.3 2.2 %fusion.5 = f32[512,512]{1,0:T(8,128)} fusion(bf16[512,2048]{1,0:T(8,128)(2,1)S(1)} %bitcast.122, bf16[1,2048,512]{2,1,0:T(8,128)(2,1)S(1)} %copy-done.9), kind=kOutput, calls=%fused_computation.13 | convolution fusion | flops 1073741824 | bytes 5242880 | tf_op jit(solution)/shard_map/dot_general | solution.py:110
  128.5 7.0 %convolution_convert_fusion = bf16[512,2048]{1,0:T(8,128)(2,1)} fusion(bf16[1,512,2048]{2,1,0:T(8,128)(2,1)} %param.23, bf16[512,2048]{1,0:T(8,128)(2,1)} %bitcast.123, bf16[1,2048,512]{2,1,0:T(8,128)(2,1)} %param.22, f32[512,512]{1,0:T(8,128)} %fusion.5), kind=kOutput, calls=%fused_computation.9 | convolution fusion | flops 2150105088 | bytes 9437184 | tf_op jit(solution)/shard_map/dot_general | solution.py:113
  135.4 5.9 %all-to-all-start.1 = ((bf16[16,32,2048]{2,1,0:T(8,128)(2,1)}), bf16[16,32,2048]{2,1,0:T(8,128)(2,1)}, u32[]{:S(2)}, u32[]{:S(2)}) async-start(bf16[16,32,2048]{2,1,0:T(8,128)(2,1)} %bitcast.121), calls=%async_computation.2 | async-start | bytes 4194304 | tf_op jit(solution)/shard_map/all_to_all | solution.py:117
  141.4 0.1 copy.24
  141.5 46.4 %all-to-all-done.1 = bf16[16,32,2048]{2,1,0:T(8,128)(2,1)} async-done(((bf16[16,32,2048]{2,1,0:T(8,128)(2,1)}), bf16[16,32,2048]{2,1,0:T(8,128)(2,1)}, u32[]{:S(2)}, u32[]{:S(2)}) %all-to-all-start.1) | async-done | bytes 2097184 | tf_op jit(solution)/shard_map/all_to_all | solution.py:117
  187.9 5.2 %gather_fusion.1 = bf16[256,2048]{1,0:T(8,128)(2,1)} fusion(bf16[512,2048]{1,0:T(8,128)(2,1)} %bitcast.24, s32[1024]{0:T(1024)S(1)} %pad_clamp_fusion), kind=kCustom, calls=%fused_computation.1 | custom fusion | bytes 2098176 | tf_op jit(solution)/shard_map/gather | solution.py:118
  193.1 3.4 %reshape.199 = f32[128,2,2048]{2,1,0:T(2,128)} reshape(bf16[256,2048]{1,0:T(8,128)(2,1)} %gather_fusion.1) | data formatting | bytes 3145728 | tf_op jit(solution)/shard_map/convert_element_type | solution.py:122
  196.5 4.8 %multiply_reduce_fusion = f32[128,2048]{1,0:T(8,128)S(1)} fusion(f32[128,2,2048]{2,1,0:T(2,128)} %reshape.199, f32[128,2]{1,0:T(8,128)S(1)} %copy.24), kind=kLoop, calls=%fused_computation.17 | loop fusion | flops 786432 | bytes 3146752 | tf_op jit(solution)/shard_map/reduce_sum | solution.py:122
  201.3 0.9 fusion.25
  (35 shorter events, 0.2 us)
Async XLA Ops:
  6.5 9.6 %copy-start = (bf16[512,2048]{1,0:T(8,128)(2,1)S(1)}, bf16[512,2048]{1,0:T(8,128)(2,1)}, u32[]{:S(2)}) copy-start(bf16[512,2048]{1,0:T(8,128)(2,1)} %param.16) | copy-start | bytes 6291460
  6.5 6.0 %copy-start.3 = (bf16[512,1,64]{0,2,1:T(8,128)(2,1)S(1)}, bf16[512,1,64]{0,2,1:T(8,128)(2,1)}, u32[]{:S(2)}) copy-start(bf16[512,1,64]{0,2,1:T(8,128)(2,1)} %param.13) | copy-start | bytes 196612
  6.5 58.6 %reduce-scatter.2.cloned.1.call-start = ((), (), s32[]{:S(2)}) async-start(), calls=%async_computation.3 | async-start | bytes 5242880 | tf_op jit(solution)/shard_map/reduce_scatter | solution.py:76
  7.5 5.0 %collective-permute-start = (bf16[2,128,1,64]{1,3,2,0:T(8,128)(2,1)S(1)}, bf16[2,128,1,64]{1,3,2,0:T(8,128)(2,1)S(1)}, u32[]{:S(2)}, u32[]{:S(2)}) collective-permute-start(bf16[2,128,1,64]{1,3,2,0:T(8,128)(2,1)S(1)} %pad_maximum_fusion.2), channel_id=1, source_target_pairs={{0,4},{4,8},{8,12},{1,5},{5,9},{9,13},{2,6},{6,10},{10,14},{3,7},{... | collective-permute-start | bytes 98312 | tf_op jit(solution)/shard_map/ppermute | solution.py:15
  12.5 0.9 copy-start.8
  13.5 1.0 copy-start.4
  19.4 0.7 copy-start.6
  19.4 45.8 %copy-start.2 = (bf16[128,2048]{1,0:T(8,128)(2,1)S(1)}, bf16[128,2048]{1,0:T(8,128)(2,1)}, u32[]{:S(2)}) copy-start(bf16[128,2048]{1,0:T(8,128)(2,1)} %param.17) | copy-start | bytes 1572868
  20.1 46.6 %copy-start.5 = (f32[2048]{0:T(1024)S(1)}, f32[2048]{0:T(1024)}, u32[]{:S(2)}) copy-start(f32[2048]{0:T(1024)} %param.18) | copy-start | bytes 24580
  72.0 54.3 %copy-start.9 = (bf16[1,2048,512]{2,1,0:T(8,128)(2,1)S(1)}, bf16[1,2048,512]{2,1,0:T(8,128)(2,1)}, u32[]{:S(2)}) copy-start(bf16[1,2048,512]{2,1,0:T(8,128)(2,1)} %param.21) | copy-start | bytes 6291460
  125.0 1.3 copy-start.1
  135.4 5.9 %copy-start.7 = (f32[128,2]{0,1:T(2,128)S(1)}, f32[128,2]{0,1:T(2,128)}, u32[]{:S(2)}) copy-start(f32[128,2]{0,1:T(2,128)} %param.20) | copy-start | bytes 3076
  135.4 52.4 %all-to-all-start.1 = ((bf16[16,32,2048]{2,1,0:T(8,128)(2,1)}), bf16[16,32,2048]{2,1,0:T(8,128)(2,1)}, u32[]{:S(2)}, u32[]{:S(2)}) async-start(bf16[16,32,2048]{2,1,0:T(8,128)(2,1)} %bitcast.121), calls=%async_computation.2 | async-start | bytes 4194304 | tf_op jit(solution)/shard_map/all_to_all | solution.py:117
Sparse Core Ops, SparseCore 0:
  19.5 45.5 reduce-scatter.1
where the time goes:
time: 211 us; the launch traced here: 209 us
  waiting for transfers between devices  86.9 us (41%)
  blocking collectives  53 us (25%)
  local copies, waits for them, and re-layouts  22.5 us (11%)
  matrix products  14.5 us (7%)
  between operations  13.6 us (6%)
  other arithmetic  11.4 us (5%)
  starting transfers between devices  7.16 us (3%)
    all_to_all x1, blocking collectives, on_device(): lax.all_to_all(outbox, ('sp', 'tp'), split_axis=0, concat_axis=0, tiled=T...  53 us
    all_to_all x1, waiting for transfers between devices, on_device(): lax.all_to_all(results, ('sp', 'tp'), split_axis=0, concat_axis=0, tiled=...  46.4 us
    reduce_scatter x1, waiting for transfers between devices, on_device(): lax.psum_scatter(jnp.dot(attended, out_weight, preferred_element_type=jnp...  40.5 us
    dot_general x1, matrix products, on_device(): jnp.dot(expert_hidden, w_down_own, preferred_element_type=jnp.float32)  6.95 us
    all_to_all x1, starting transfers between devices, on_device(): lax.all_to_all(results, ('sp', 'tp'), split_axis=0, concat_axis=0, tiled=...  5.87 us
    gather x1, local copies, waits for them, and re-layouts, on_device(): returned.reshape(experts_total * capacity, width)[flat_slot]  5.2 us
    reduce_sum x1, other arithmetic, on_device(): jnp.sum(shares[:, :, None] * picked_rows.astype(jnp.float32), axis=1)  4.81 us
  transfers between devices with their start and end apart: 3, of which 2 were waited for; matrix products, arithmetic and copies ran while one was open for 4% of the time, Pallas kernels for 0%

commit v1 on v0

--- a/solution.py
+++ b/solution.py
@@ -1,12 +1,21 @@
+import functools
+
 import jax
 import jax.numpy as jnp
 from jax import lax
+from jax.experimental import pallas as pl
+from jax.experimental.pallas import tpu as pltpu
 from jax.sharding import PartitionSpec as P
 
 WINDOW = 128
 
 
 EPS = 1e-06
+
+F32 = jnp.float32
+BF16 = jnp.bfloat16
+MESH = pl.DeviceIdType.MESH
+VMEM_BUDGET = 56 * 1024 * 1024
 
 
 def from_behind(value, axis, steps):
@@ -15,20 +24,11 @@
     return lax.ppermute(value, axis, [(source, source + steps) for source in range(initial, last)])
 
 
-def on_device(
-    queries,
-    key_heads,
-    value_heads,
-    sink_logit,
-    out_weight,
-    residual,
-    norm_gain,
-    expert_ids,
-    route_weights,
-    gate_weight,
-    up_weight,
-    down_weight,
-):
+def dot(a, b, dims=((1,), (0,))):
+    return lax.dot_general(a, b, (dims, ((), ())), preferred_element_type=F32)
+
+
+def attention(queries, key_heads, value_heads, sink_logit):
     rows_sp = queries.shape[0]
     kv_local = key_heads.shape[1]
     head_dim = key_heads.shape[2]
@@ -70,7 +70,13 @@
     attended = jnp.einsum(
         "bhgqk,bkhd->bqhgd", attention_probabilities, value_span, preferred_element_type=jnp.float32
     ).astype(jnp.bfloat16)
-    attended = attended.reshape(rows_sp, heads_local * head_dim)
+    return attended.reshape(rows_sp, heads_local * head_dim)
+
+
+def tail_plain(
+    attended, out_weight, residual, norm_gain, expert_ids, route_weights,
+    gate_weight, up_weight, down_weight,
+):
     rows_dev = residual.shape[0]
     width = residual.shape[1]
     projected = lax.psum_scatter(
@@ -102,15 +108,12 @@
     filled = jnp.zeros((experts_total * capacity,), jnp.bool_).at[flat_slot].set(True)
     outbox = jnp.where(filled[:, None], normed[token_in_slot], jnp.zeros((), jnp.bfloat16))
     outbox = outbox.reshape(experts_total, capacity, width)
-    w_gate_own = gate_weight[0]
-    w_up_own = up_weight[0]
-    w_down_own = down_weight[0]
     arrived = lax.all_to_all(outbox, ("sp", "tp"), split_axis=0, concat_axis=0, tiled=True)
     rows = arrived.reshape(-1, width)
-    gate = jnp.dot(rows, w_gate_own, preferred_element_type=jnp.float32)
-    upward = jnp.dot(rows, w_up_own, preferred_element_type=jnp.float32)
+    gate = jnp.dot(rows, gate_weight[0], preferred_element_type=jnp.float32)
+    upward = jnp.dot(rows, up_weight[0], preferred_element_type=jnp.float32)
     expert_hidden = (jax.nn.silu(gate) * upward).astype(jnp.bfloat16)
-    expert_rows = jnp.dot(expert_hidden, w_down_own, preferred_element_type=jnp.float32).astype(
+    expert_rows = jnp.dot(expert_hidden, down_weight[0], preferred_element_type=jnp.float32).astype(
         jnp.bfloat16
     )
     results = expert_rows.reshape(arrived.shape)
@@ -121,6 +124,279 @@
     shares = route_weights / jnp.sum(route_weights, axis=-1, keepdims=True)
     combined = jnp.sum(shares[:, :, None] * picked_rows.astype(jnp.float32), axis=1)
     return (wide + combined).astype(jnp.bfloat16)
+
+
+def routing(ids, weights, experts, capacity):
+    rows, top_k = ids.shape
+    expert = lax.broadcasted_iota(jnp.int32, (rows, experts), 1)
+    total = jnp.sum(weights, axis=1, keepdims=True)
+    member = jnp.zeros((rows, experts), F32)
+    share = jnp.zeros((rows, experts), F32)
+    for k in range(top_k):
+        hit = (ids[:, k : k + 1] == expert).astype(F32)
+        member = member + hit
+        share = share + hit * (weights[:, k : k + 1] / total)
+    before = (
+        lax.broadcasted_iota(jnp.int32, (rows, rows), 0)
+        > lax.broadcasted_iota(jnp.int32, (rows, rows), 1)
+    ).astype(BF16)
+    rank = dot(before, member.astype(BF16))
+    rank = jnp.where(member > 0, rank, -1.0)
+    slots = experts * capacity
+    spread = (
+        lax.broadcasted_iota(jnp.int32, (experts, slots), 1) // capacity
+        == lax.broadcasted_iota(jnp.int32, (experts, slots), 0)
+    ).astype(BF16)
+    rank_slot = dot(rank.astype(BF16), spread)
+    place = lax.broadcasted_iota(jnp.int32, (rows, slots), 1) % capacity
+    taken = rank_slot == place.astype(F32)
+    high = share.astype(BF16)
+    low = (share - high.astype(F32)).astype(BF16)
+    one = jnp.where(taken, 1.0, 0.0)
+    return (
+        one.astype(BF16),
+        (one * dot(high, spread)).astype(BF16),
+        (one * dot(low, spread)).astype(BF16),
+    )
+
+
+def tail_kernel(
+    sizes,
+    attended, out_w_hbm, residual, gain, ids, weights, gate_hbm, up_hbm, down_hbm,
+    out,
+    out_w, gate_w, up_w, down_w,
+    pair_out, pair_in, far_out, far_in,
+    stream, normed, slots, share_hi, share_lo,
+    outbox, arrived, results, returned,
+    load_sem, pair_send, pair_recv, far_send, far_recv,
+    go_send, go_recv, back_send, back_recv,
+):
+    sp_count, tp_count, pieces, capacity = sizes
+    experts = sp_count * tp_count
+    chips = tp_count // 2
+    z, t = lax.axis_index("sp"), lax.axis_index("tp")
+    me = z * tp_count + t
+    x, core = t // 2, t % 2
+    other = 1 - core
+    rows, width = residual.shape
+    piece = width // pieces
+
+    def where(e):
+        return {"sp": e // tp_count, "tp": e % tp_count}
+
+    loads = [
+        pltpu.make_async_copy(src, dst, load_sem.at[i])
+        for i, (src, dst) in enumerate(
+            ((out_w_hbm, out_w), (gate_hbm.at[0], gate_w), (up_hbm.at[0], up_w), (down_hbm.at[0], down_w))
+        )
+    ]
+    for load in loads:
+        load.start()
+
+    barrier = pltpu.get_barrier_semaphore()
+
+    def greet(k, carry):
+        pl.semaphore_signal(
+            barrier, inc=1, device_id=where((me + k) % experts), device_id_type=MESH
+        )
+        return carry
+
+    lax.fori_loop(1, experts, greet, 0)
+    slots[...], share_hi[...], share_lo[...] = routing(ids[...], weights[...], experts, capacity)
+    loads[0].wait()
+    pl.semaphore_wait(barrier, experts - 1)
+
+    def partial(chip, which, q):
+        block = attended[pl.ds(pl.multiple_of((chip * 2 + which) * rows, rows), rows), :]
+        return dot(block, out_w[:, q * piece : (q + 1) * piece])
+
+    def pair_copy(k, q):
+        return pltpu.make_async_remote_copy(
+            pair_out.at[k, q], pair_in.at[k, q], pair_send.at[k, q], pair_recv.at[k, q],
+            device_id={"tp": x * 2 + other}, device_id_type=MESH,
+        )
+
+    def far_copy(k, q):
+        return pltpu.make_async_remote_copy(
+            far_out.at[k, q], far_in.at[k, q], far_send.at[k, q], far_recv.at[k, q],
+            device_id={"tp": ((x + k) % chips) * 2 + core}, device_id_type=MESH,
+        )
+
+    order = list(range(1, chips)) + [0]
+    for q in range(pieces):
+        for k in order:
+            pair_out[k, q] = partial((x + k) % chips, other, q).astype(BF16)
+            pair_copy(k, q).start()
+        for k in range(1, chips):
+            mine = partial((x + k) % chips, core, q)
+            pair_copy(k, q).wait_recv()
+            far_out[k, q] = (mine + pair_in[k, q].astype(F32)).astype(BF16)
+            far_copy(k, q).start()
+    square = jnp.zeros((rows, 1), F32)
+    for q in range(pieces):
+        cols = slice(q * piece, (q + 1) * piece)
+        total = partial(x, core, q)
+        pair_copy(0, q).wait_recv()
+        total = total + pair_in[0, q].astype(F32)
+        for k in range(1, chips):
+            far_copy(k, q).wait_recv()
+            total = total + far_in[k, q].astype(F32)
+        value = (residual[:, cols].astype(F32) + total).astype(BF16)
+        stream[:, cols] = value
+        value = value.astype(F32)
+        square = square + jnp.sum(value * value, axis=1, keepdims=True)
+    scale = lax.rsqrt(square / width + EPS)
+    for q in range(pieces):
+        cols = slice(q * piece, (q + 1) * piece)
+        normed[:, cols] = (stream[:, cols].astype(F32) * scale * gain[:, cols]).astype(BF16)
+
+    def go_copy(to, at):
+        return pltpu.make_async_remote_copy(
+            outbox.at[to], arrived.at[at], go_send.at[to], go_recv.at[at],
+            device_id=where(to), device_id_type=MESH,
+        )
+
+    def back_copy(to, at):
+        return pltpu.make_async_remote_copy(
+            results.at[to], returned.at[at], back_send.at[to], back_recv.at[at],
+            device_id=where(to), device_id_type=MESH,
+        )
+
+    picks = tp_count * capacity
+    for d in range(sp_count):
+        layer = range(d * tp_count, (d + 1) * tp_count)
+        chosen = dot(slots[:, d * picks : (d + 1) * picks], normed[...], ((0,), (0,))).astype(BF16)
+        for i, e in enumerate(layer):
+            outbox[e] = chosen[i * capacity : (i + 1) * capacity]
+
+            @pl.when(e != me)
+            def _():
+                go_copy(e, me).start()
+
+    arrived[me] = outbox[me]
+    for load in loads[1:]:
+        load.wait()
+
+    def expert(d, carry):
+        layer = (z + d) % sp_count
+        for i in range(tp_count):
+            e = layer * tp_count + i
+
+            @pl.when(e != me)
+            def _():
+                go_copy(me, e).wait_recv()
+
+        block = arrived[pl.ds(layer * tp_count, tp_count)].reshape(picks, width)
+        gated = dot(block, gate_w[...])
+        raised = dot(block, up_w[...])
+        hidden = (gated / (1.0 + jnp.exp(-gated)) * raised).astype(BF16)
+        done = dot(hidden, down_w[...]).astype(BF16)
+        results[pl.ds(layer * tp_count, tp_count)] = done.reshape(tp_count, capacity, width)
+        for i in range(tp_count):
+            e = layer * tp_count + i
+
+            @pl.when(e != me)
+            def _():
+                back_copy(e, me).start()
+
+        return carry
+
+    lax.fori_loop(0, sp_count, expert, 0)
+    returned[me] = results[me]
+
+    def collect(k, carry):
+        e = (me + k) % experts
+        back_copy(me, e).wait_recv()
+        return carry
+
+    lax.fori_loop(1, experts, collect, 0)
+    for q in range(pieces):
+        cols = slice(q * piece, (q + 1) * piece)
+        back = returned[:, :, cols].reshape(experts * capacity, piece)
+        mixed = dot(share_hi[...], back) + dot(share_lo[...], back)
+        out[:, cols] = (stream[:, cols].astype(F32) + mixed).astype(BF16)
+
+    for q in range(pieces):
+        for k in range(chips):
+            pair_copy(k, q).wait_send()
+            if k:
+                far_copy(k, q).wait_send()
+
+    def flush(k, carry):
+        e = (me + k) % experts
+        go_copy(e, me).wait_send()
+        back_copy(e, me).wait_send()
+        return carry
+
+    lax.fori_loop(1, experts, flush, 0)
+
+
+def tail_fused(
+    attended, out_weight, residual, norm_gain, expert_ids, route_weights,
+    gate_weight, up_weight, down_weight,
+):
+    rows, width = residual.shape
+    sp_count, tp_count = lax.axis_size("sp"), lax.axis_size("tp")
+    experts = sp_count * tp_count
+    top_k = expert_ids.shape[1]
+    capacity = max(2, 2 * top_k * rows // experts)
+    hidden = gate_weight.shape[2]
+    depth = out_weight.shape[0]
+    pieces = 4
+    chips = tp_count // 2
+    part = (chips, pieces, rows, width // pieces)
+    box = (experts, capacity, width)
+    vmem = pl.BlockSpec(memory_space=pltpu.VMEM)
+    hbm = pl.BlockSpec(memory_space=pl.ANY)
+    dma = pltpu.SemaphoreType.DMA
+    return pl.pallas_call(
+        functools.partial(tail_kernel, (sp_count, tp_count, pieces, capacity)),
+        out_shape=jax.ShapeDtypeStruct((rows, width), BF16),
+        in_specs=[vmem, hbm, vmem, vmem, vmem, vmem, hbm, hbm, hbm],
+        out_specs=vmem,
+        scratch_shapes=[
+            pltpu.VMEM((depth, width), BF16),
+            pltpu.VMEM((width, hidden), BF16),
+            pltpu.VMEM((width, hidden), BF16),
+            pltpu.VMEM((hidden, width), BF16),
+            pltpu.VMEM(part, BF16),
+            pltpu.VMEM(part, BF16),
+            pltpu.VMEM(part, BF16),
+            pltpu.VMEM(part, BF16),
+            pltpu.VMEM((rows, width), BF16),
+            pltpu.VMEM((rows, width), BF16),
+            pltpu.VMEM((rows, experts * capacity), BF16),
+            pltpu.VMEM((rows, experts * capacity), BF16),
+            pltpu.VMEM((rows, experts * capacity), BF16),
+            pltpu.VMEM(box, BF16),
+            pltpu.VMEM(box, BF16),
+            pltpu.VMEM(box, BF16),
+            pltpu.VMEM(box, BF16),
+            dma((4,)),
+            dma((chips, pieces)),
+            dma((chips, pieces)),
+            dma((chips, pieces)),
+            dma((chips, pieces)),
+            dma((experts,)),
+            dma((experts,)),
+            dma((experts,)),
+            dma((experts,)),
+        ],
+        compiler_params=pltpu.CompilerParams(
+            collective_id=0, has_side_effects=True, vmem_limit_bytes=VMEM_BUDGET
+        ),
+    )(
+        attended, out_weight, residual, norm_gain[None], expert_ids, route_weights,
+        gate_weight, up_weight, down_weight,
+    )
+
+
+def on_device(queries, key_heads, value_heads, sink_logit, *rest):
+    attended = attention(queries, key_heads, value_heads, sink_logit)
+    rows_dev = rest[1].shape[0]
+    experts = lax.axis_size("sp") * lax.axis_size("tp")
+    fits = 2 * rest[3].shape[1] * rows_dev // experts % 16 == 0
+    return (tail_fused if fits else tail_plain)(attended, *rest)
 
 
 def solution(mesh):

time: 211 us -> 135 us (0.64)
  Pallas kernels: 0 us -> 118 us
  waiting for transfers between devices: 86.9 us -> 0.01 us
  blocking collectives: 53 us -> 0 us
  between operations: 13.6 us -> 0.12 us
  matrix products: 14.5 us -> 2.08 us
  local copies, waits for them, and re-layouts: 22.5 us -> 10.8 us
  other arithmetic: 11.4 us -> 2.24 us
  starting transfers between devices: 7.16 us -> 1.28 us
    pallas_call x0 -> x1, Pallas kernels: none -> 118 us  [tail_fused(): pl.pallas_call(functools.partial(tail_kernel, (sp_count, tp_count, pieces...]
    all_to_all x1 -> x0, blocking collectives: 53 us -> none  [on_device(): lax.all_to_all(outbox, ('sp', 'tp'), split_axis=0, concat_axis=0, tiled=T...]
    all_to_all x1 -> x0, waiting for transfers between devices: 46.4 us -> none  [on_device(): lax.all_to_all(results, ('sp', 'tp'), split_axis=0, concat_axis=0, tiled=...]
    reduce_scatter x1 -> x0, waiting for transfers between devices: 40.5 us -> none  [on_device(): lax.psum_scatter(jnp.dot(attended, out_weight, preferred_element_type=jnp...]
    dot_general x5 -> x2, matrix products: 14.5 us -> 2.08 us  [the longest x1 1.19 us: attention(): jnp.einsum('bhgqk,bkhd->bqhgd', attention_probabilities, value_span, pref...]
    gather x2 -> x0, local copies, waits for them, and re-layouts: 8.55 us -> none  [the longest x1 5.2 us: on_device(): returned.reshape(experts_total * capacity, width)[flat_slot]]
    reduce_sum x5 -> x1, other arithmetic: 7.32 us -> 0.93 us  [attention(): jnp.sum(expd, axis=-1, keepdims=True) + jnp.exp(sink_col - row_max)]
    all_to_all x1 -> x0, starting transfers between devices: 5.87 us -> none  [on_device(): lax.all_to_all(results, ('sp', 'tp'), split_axis=0, concat_axis=0, tiled=...]
  transfers between devices with their start and end apart: 3 -> 1, of which waited for: 2 -> 0; matrix products, arithmetic and copies ran while one was open for 4% -> 5% of each run, Pallas kernels for 0% -> 0%
where the time goes in v1:
time: 135 us; the launch traced here: 134 us
  Pallas kernels  118 us (87%)
  local copies, waits for them, and re-layouts  10.8 us (8%)
  other arithmetic  2.24 us (2%)
  matrix products  2.08 us (2%)
    pallas_call x1, Pallas kernels, tail_fused(): pl.pallas_call(functools.partial(tail_kernel, (sp_count, tp_count, pieces...  118 us
    unnamed x7, local copies, waits for them, and re-layouts  4.73 us
  transfers between devices with their start and end apart: 1, of which 0 were waited for; matrix products, arithmetic and copies ran while one was open for 5% of the time, Pallas kernels for 0%

profile of v1, /device:TPU:31, one launch (start us, length us, event | category | flops | bytes accessed | tf_op | source)
XLA Modules:
  0.0 134.1 jit_solution(11344048538742296456)
XLA Ops:
  0.0 0.0 copy-start.1
  0.0 0.7 slice_bitcast_fusion.2
  0.8 1.3 collective-permute-start
  2.1 0.9 copy_bitcast_fusion
  3.0 0.1 add_compare_fusion
  3.1 0.2 broadcast_and_fusion
  3.3 0.9 copy_bitcast_fusion.2
  4.1 1.6 %reshape.120 = bf16[4,128,8,64]{3,2,1,0:T(8,128)(2,1)S(1)} reshape(bf16[512,512]{1,0:T(8,128)(2,1)} %param.12) | data formatting | bytes 1048576 | tf_op jit(solution)/shard_map/reshape.10
  5.8 1.4 %copy.27.ids = s32[128,2]{1,0:T(8,128)} copy(s32[128,2]{0,1:T(2,128)} %param.19) | data formatting | bytes 2048 | tf_op args[7]
  7.2 1.4 %copy.28.weights = f32[128,2]{1,0:T(8,128)} copy(f32[128,2]{0,1:T(2,128)} %param.20) | data formatting | bytes 2048 | tf_op args[8]
  8.6 0.0 collective-permute-done
  8.6 0.8 copy_bitcast_fusion.1
  9.4 0.0 copy-start
  9.5 0.9 fusion.1
  10.3 0.0 copy-done.1
  10.4 0.1 broadcast_maximum_fusion
  10.4 0.9 fusion
  11.4 0.1 exponential_add_fusion
  11.4 0.0 copy-done
  11.5 1.2 fusion.8
  12.7 0.6 copy.34
  13.2 1.4 %reshape.121.attended = bf16[512,512]{1,0:T(8,128)(2,1)} reshape(bf16[4,128,1,8,64]{4,3,1,0,2:T(8,128)(2,1)S(1)} %copy.34) | data formatting | bytes 1048576 | tf_op jit(solution)/shard_map/reshape | solution.py:73
  14.6 117.6 %shard_map.118 = bf16[128,2048]{1,0:T(8,128)(2,1)} custom-call(bf16[512,512]{1,0:T(8,128)(2,1)} %reshape.121.attended, bf16[512,2048]{1,0:T(8,128)(2,1)} %out_w_hbm.1, bf16[128,2048]{1,0:T(8,128)(2,1)} %residual.1, f32[1,2048]{1,0:T(1,128)} %bitcast.75, s32[128,2]{1,0:T(8,128)} %copy.27.ids, f32[128,2]{1,0:T(8,128)} %copy.28.weights, ...), custom_call_target="tpu_custom_call" | custom-call | tf_op jit(solution)/shard_map/pallas_call | solution.py:352
  132.2 1.9 %copy.49 = bf16[128,2048]{1,0:T(8,128)(2,1)} copy(bf16[128,2048]{1,0:T(8,128)(2,1)} %shard_map.118) | data formatting | bytes 1048576
  (6 shorter events, 0.1 us)
Async XLA Ops:
  0.0 10.3 %copy-start.1 = (f32[8]{0:T(128)S(1)}, f32[8]{0:T(128)}, u32[]{:S(2)}) copy-start(f32[8]{0:T(128)} %param.15) | copy-start | bytes 100
  0.8 7.9 %collective-permute-start = (bf16[2,128,1,64]{1,3,2,0:T(8,128)(2,1)S(1)}, bf16[2,128,1,64]{1,3,2,0:T(8,128)(2,1)S(1)}, u32[]{:S(2)}, u32[]{:S(2)}) collective-permute-start(bf16[2,128,1,64]{1,3,2,0:T(8,128)(2,1)S(1)} %pad_maximum_fusion.2), channel_id=1, source_target_pairs={{0,4},{4,8},{8,12},{1,5},{5,9},{9,13},{2,6},{6,10},{10,14},{3,7},{... | collective-permute-start | bytes 98312 | tf_op jit(solution)/shard_map/ppermute | solution.py:24
  9.4 2.0 %copy-start = (bf16[512,1,64]{0,2,1:T(8,128)(2,1)S(1)}, bf16[512,1,64]{0,2,1:T(8,128)(2,1)}, u32[]{:S(2)}) copy-start(bf16[512,1,64]{0,2,1:T(8,128)(2,1)} %param.14) | copy-start | bytes 196612

commit v2 on v1

--- a/solution.py
+++ b/solution.py
@@ -160,10 +160,75 @@
     )
 
 
+def attend(sp_count, z, queries, kv, sink, halo, attended, send, recv):
+    rows, lanes = kv.shape
+    window = halo.shape[0]
+    heads = sink.shape[1]
+    size = queries.shape[1] // heads
+    groups = lanes // (2 * size)
+    share = heads // groups
+    copy = pltpu.make_async_remote_copy(
+        kv.at[pl.ds(rows - window, window)], halo, send, recv,
+        device_id={"sp": jnp.minimum(z + 1, sp_count - 1)}, device_id_type=MESH,
+    )
+
+    @pl.when(z < sp_count - 1)
+    def _():
+        copy.start()
+
+    distance = (
+        lax.broadcasted_iota(jnp.int32, (window, 2 * window), 0)
+        + window
+        - lax.broadcasted_iota(jnp.int32, (window, 2 * window), 1)
+    )
+    band = (distance >= 0) & (distance < window)
+    key = lax.broadcasted_iota(jnp.int32, (window, 2 * window), 1)
+
+    def block(b):
+        allowed = band
+        if b == 0:
+            allowed = band & (z * rows - window + key >= 0)
+            span = jnp.concatenate([halo[...], kv[:window]], 0)
+        else:
+            span = kv[(b - 1) * window : (b + 1) * window]
+        here = slice(b * window, (b + 1) * window)
+        done = []
+        for h in range(heads):
+            g = h // share
+            keys = span[:, 2 * g * size : (2 * g + 1) * size]
+            values = span[:, (2 * g + 1) * size : (2 * g + 2) * size]
+            score = dot(queries[here, h * size : (h + 1) * size], keys, ((1,), (1,))) * size**-0.5
+            score = jnp.where(allowed, score, -1e30)
+            drain = sink[0:1, h : h + 1]
+            top = jnp.maximum(jnp.max(score, axis=1, keepdims=True), drain)
+            grown = jnp.exp(score - top)
+            total = jnp.sum(grown, axis=1, keepdims=True) + jnp.exp(drain - top)
+            done.append(dot((grown * (1.0 / total)).astype(BF16), values).astype(BF16))
+        attended[here, :] = jnp.concatenate(done, 1)
+
+    for b in range(1, rows // window):
+        block(b)
+
+    @pl.when(z == 0)
+    def _():
+        halo[...] = jnp.zeros_like(halo)
+
+    @pl.when(z > 0)
+    def _():
+        copy.wait_recv()
+
+    block(0)
+
+    @pl.when(z < sp_count - 1)
+    def _():
+        copy.wait_send()
+
+
 def tail_kernel(
     sizes,
-    attended, out_w_hbm, residual, gain, ids, weights, gate_hbm, up_hbm, down_hbm,
+    queries, kv, sink, out_w_hbm, residual, gain, ids, weights, gate_hbm, up_hbm, down_hbm,
     out,
+    halo, attended, halo_send, halo_recv,
     out_w, gate_w, up_w, down_w,
     pair_out, pair_in, far_out, far_in,
     stream, normed, slots, share_hi, share_lo,
@@ -202,9 +267,9 @@
         return carry
 
     lax.fori_loop(1, experts, greet, 0)
-    slots[...], share_hi[...], share_lo[...] = routing(ids[...], weights[...], experts, capacity)
+    pl.semaphore_wait(barrier, experts - 1)
+    attend(sp_count, z, queries, kv, sink, halo, attended, halo_send, halo_recv)
     loads[0].wait()
-    pl.semaphore_wait(barrier, experts - 1)
 
     def partial(chip, which, q):
         block = attended[pl.ds(pl.multiple_of((chip * 2 + which) * rows, rows), rows), :]
@@ -232,6 +297,7 @@
             pair_copy(k, q).wait_recv()
             far_out[k, q] = (mine + pair_in[k, q].astype(F32)).astype(BF16)
             far_copy(k, q).start()
+    slots[...], share_hi[...], share_lo[...] = routing(ids[...], weights[...], experts, capacity)
     square = jnp.zeros((rows, 1), F32)
     for q in range(pieces):
         cols = slice(q * piece, (q + 1) * piece)
@@ -331,8 +397,8 @@
     lax.fori_loop(1, experts, flush, 0)
 
 
-def tail_fused(
-    attended, out_weight, residual, norm_gain, expert_ids, route_weights,
+def fused(
+    queries, key_heads, value_heads, sink_logit, out_weight, residual, norm_gain, expert_ids, route_weights,
     gate_weight, up_weight, down_weight,
 ):
     rows, width = residual.shape
@@ -346,15 +412,21 @@
     chips = tp_count // 2
     part = (chips, pieces, rows, width // pieces)
     box = (experts, capacity, width)
+    seen, groups, size = key_heads.shape
+    kv = jnp.stack([key_heads, value_heads], 2).reshape(seen, groups * 2 * size)
     vmem = pl.BlockSpec(memory_space=pltpu.VMEM)
     hbm = pl.BlockSpec(memory_space=pl.ANY)
     dma = pltpu.SemaphoreType.DMA
     return pl.pallas_call(
         functools.partial(tail_kernel, (sp_count, tp_count, pieces, capacity)),
         out_shape=jax.ShapeDtypeStruct((rows, width), BF16),
-        in_specs=[vmem, hbm, vmem, vmem, vmem, vmem, hbm, hbm, hbm],
+        in_specs=[vmem, vmem, vmem, hbm, vmem, vmem, vmem, vmem, hbm, hbm, hbm],
         out_specs=vmem,
         scratch_shapes=[
+            pltpu.VMEM((WINDOW, kv.shape[1]), BF16),
+            pltpu.VMEM(queries.shape, BF16),
+            dma,
+            dma,
             pltpu.VMEM((depth, width), BF16),
             pltpu.VMEM((width, hidden), BF16),
             pltpu.VMEM((width, hidden), BF16),
@@ -386,17 +458,18 @@
             collective_id=0, has_side_effects=True, vmem_limit_bytes=VMEM_BUDGET
         ),
     )(
-        attended, out_weight, residual, norm_gain[None], expert_ids, route_weights,
+        queries, kv, sink_logit[None], out_weight, residual, norm_gain[None], expert_ids, route_weights,
         gate_weight, up_weight, down_weight,
     )
 
 
 def on_device(queries, key_heads, value_heads, sink_logit, *rest):
-    attended = attention(queries, key_heads, value_heads, sink_logit)
     rows_dev = rest[1].shape[0]
     experts = lax.axis_size("sp") * lax.axis_size("tp")
     fits = 2 * rest[3].shape[1] * rows_dev // experts % 16 == 0
-    return (tail_fused if fits else tail_plain)(attended, *rest)
+    if fits:
+        return fused(queries, key_heads, value_heads, sink_logit, *rest)
+    return tail_plain(attention(queries, key_heads, value_heads, sink_logit), *rest)
 
 
 def solution(mesh):

time: 135 us -> 136 us (level)
  Pallas kernels: 118 us -> 129 us
  local copies, waits for them, and re-layouts: 10.8 us -> 5.45 us
  matrix products: 2.08 us -> 0 us
  other arithmetic: 2.24 us -> 0.88 us
    pallas_call x1, Pallas kernels: 118 us -> 129 us  [fused(): pl.pallas_call(functools.partial(tail_kernel, (sp_count, tp_count, pieces...]
    another operation x2 -> x0, local copies, waits for them, and re-layouts: 2.4 us -> none
    dot_general x2 -> x0, matrix products: 2.08 us -> none  [the longest x1 1.19 us: attention(): jnp.einsum('bhgqk,bkhd->bqhgd', attention_probabilities, value_span, pref...]
    slice x2 -> x0, local copies, waits for them, and re-layouts: 1.71 us -> none  [the longest x1 0.85 us: attention(): value_span = jnp.concatenate([value_blocks[:-1], value_blocks[1:]], 1)]
    unnamed x7 -> x3, local copies, waits for them, and re-layouts: 4.73 us -> 4.69 us
  transfers between devices with their start and end apart: 1 -> 0, of which waited for: 0 -> 0; matrix products, arithmetic and copies ran while one was open for 5% -> 0% of each run, Pallas kernels for 0% -> 0%
where the time goes in v2:
time: 136 us; the launch traced here: 135 us
  Pallas kernels  129 us (95%)
  local copies, waits for them, and re-layouts  5.45 us (4%)
    pallas_call x1, Pallas kernels, fused(): pl.pallas_call(functools.partial(tail_kernel, (sp_count, tp_count, pieces...  129 us
    unnamed x3, local copies, waits for them, and re-layouts  4.69 us

profile of v2, /device:TPU:31, one launch (start us, length us, event | category | flops | bytes accessed | tf_op | source)
XLA Modules:
  0.0 135.3 jit_solution(6591015932838913548)
XLA Ops:
  0.0 1.4 %copy.17.ids = s32[128,2]{1,0:T(8,128)} copy(s32[128,2]{0,1:T(2,128)} %param.19) | data formatting | bytes 2048 | tf_op args[7]
  1.4 1.4 %copy.18.weights = f32[128,2]{1,0:T(8,128)} copy(f32[128,2]{0,1:T(2,128)} %param.20) | data formatting | bytes 2048 | tf_op args[8]
  2.8 0.9 pad_maximum_fusion
  3.7 0.8 copy.16.kv
  4.5 128.9 %shard_map.118 = bf16[128,2048]{1,0:T(8,128)(2,1)} custom-call(bf16[512,512]{1,0:T(8,128)(2,1)} %queries.1, bf16[512,128]{1,0:T(8,128)(2,1)} %copy.16.kv, f32[1,8]{1,0:T(1,128)} %bitcast.9, bf16[512,2048]{1,0:T(8,128)(2,1)} %out_w_hbm.1, bf16[128,2048]{1,0:T(8,128)(2,1)} %residual.1, f32[1,2048]{1,0:T(1,128)} %bitcast.8, s32[128,2]{1,0:T(8,128)} %copy.17.ids, ...), custom_call_target="tpu_custom_call" | custom-call | tf_op jit(solution)/shard_map/pallas_call | solution.py:420
  133.4 1.9 %copy.20 = bf16[128,2048]{1,0:T(8,128)(2,1)} copy(bf16[128,2048]{1,0:T(8,128)(2,1)} %shard_map.118) | data formatting | bytes 1048576

commit v3 on v2

--- a/solution.py
+++ b/solution.py
@@ -176,13 +176,12 @@
     def _():
         copy.start()
 
-    distance = (
-        lax.broadcasted_iota(jnp.int32, (window, 2 * window), 0)
-        + window
-        - lax.broadcasted_iota(jnp.int32, (window, 2 * window), 1)
-    )
+    pairs = share // 2
+    tall = pairs * window
+    query = lax.broadcasted_iota(jnp.int32, (tall, 2 * window), 0) % window
+    key = lax.broadcasted_iota(jnp.int32, (tall, 2 * window), 1)
+    distance = query + window - key
     band = (distance >= 0) & (distance < window)
-    key = lax.broadcasted_iota(jnp.int32, (window, 2 * window), 1)
 
     def block(b):
         allowed = band
@@ -192,19 +191,44 @@
         else:
             span = kv[(b - 1) * window : (b + 1) * window]
         here = slice(b * window, (b + 1) * window)
-        done = []
-        for h in range(heads):
-            g = h // share
+        for g in range(groups):
             keys = span[:, 2 * g * size : (2 * g + 1) * size]
             values = span[:, (2 * g + 1) * size : (2 * g + 2) * size]
-            score = dot(queries[here, h * size : (h + 1) * size], keys, ((1,), (1,))) * size**-0.5
-            score = jnp.where(allowed, score, -1e30)
-            drain = sink[0:1, h : h + 1]
-            top = jnp.maximum(jnp.max(score, axis=1, keepdims=True), drain)
-            grown = jnp.exp(score - top)
-            total = jnp.sum(grown, axis=1, keepdims=True) + jnp.exp(drain - top)
-            done.append(dot((grown * (1.0 / total)).astype(BF16), values).astype(BF16))
-        attended[here, :] = jnp.concatenate(done, 1)
+            none, ones = jnp.zeros_like(keys), jnp.ones_like(values)
+            wide = jnp.concatenate(
+                [
+                    queries[here, (g * share + 2 * i) * size : (g * share + 2 * i + 2) * size]
+                    for i in range(pairs)
+                ],
+                0,
+            )
+            sides = []
+            for odd in range(2):
+                two_keys = jnp.concatenate([none, keys] if odd else [keys, none], 1)
+                two_values = jnp.concatenate([ones, values] if odd else [values, ones], 1)
+                score = dot(wide, two_keys, ((1,), (1,))) * size**-0.5
+                score = jnp.where(allowed, score, -1e30)
+                drain = jnp.concatenate(
+                    [
+                        jnp.broadcast_to(
+                            sink[0:1, g * share + 2 * i + odd : g * share + 2 * i + odd + 1],
+                            (window, 1),
+                        )
+                        for i in range(pairs)
+                    ],
+                    0,
+                )
+                top = jnp.maximum(jnp.max(score, axis=1, keepdims=True), drain)
+                grown = jnp.exp(score - top).astype(BF16)
+                both = dot(grown, two_values)
+                at = 0 if odd else size
+                total = both[:, at : at + 1] + jnp.exp(drain - top)
+                sides.append(both * (1.0 / total))
+            lane = lax.broadcasted_iota(jnp.int32, (tall, 2 * size), 1)
+            both = jnp.where(lane < size, sides[0], sides[1]).astype(BF16)
+            for i in range(pairs):
+                first = (g * share + 2 * i) * size
+                attended[here, first : first + 2 * size] = both[i * window : (i + 1) * window]
 
     for b in range(1, rows // window):
         block(b)

time: 136 us -> 129 us (0.949)
  Pallas kernels: 129 us -> 122 us
    pallas_call x1, Pallas kernels: 129 us -> 122 us  [fused(): pl.pallas_call(functools.partial(tail_kernel, (sp_count, tp_count, pieces...]
where the time goes in v3:
time: 129 us; the launch traced here: 128 us
  Pallas kernels  122 us (95%)
  local copies, waits for them, and re-layouts  5.45 us (4%)
    pallas_call x1, Pallas kernels, fused(): pl.pallas_call(functools.partial(tail_kernel, (sp_count, tp_count, pieces...  122 us
    unnamed x3, local copies, waits for them, and re-layouts  4.69 us

profile of v3, /device:TPU:31, one launch (start us, length us, event | category | flops | bytes accessed | tf_op | source)
XLA Modules:
  0.0 128.5 jit_solution(7238292065867759286)
XLA Ops:
  0.0 1.4 %copy.17.ids = s32[128,2]{1,0:T(8,128)} copy(s32[128,2]{0,1:T(2,128)} %param.19) | data formatting | bytes 2048 | tf_op args[7]
  1.4 1.4 %copy.18.weights = f32[128,2]{1,0:T(8,128)} copy(f32[128,2]{0,1:T(2,128)} %param.20) | data formatting | bytes 2048 | tf_op args[8]
  2.8 0.9 pad_maximum_fusion
  3.7 0.8 copy.16.kv
  4.5 122.1 %shard_map.118 = bf16[128,2048]{1,0:T(8,128)(2,1)} custom-call(bf16[512,512]{1,0:T(8,128)(2,1)} %queries.1, bf16[512,128]{1,0:T(8,128)(2,1)} %copy.16.kv, f32[1,8]{1,0:T(1,128)} %bitcast.9, bf16[512,2048]{1,0:T(8,128)(2,1)} %out_w_hbm.1, bf16[128,2048]{1,0:T(8,128)(2,1)} %residual.1, f32[1,2048]{1,0:T(1,128)} %bitcast.8, s32[128,2]{1,0:T(8,128)} %copy.17.ids, ...), custom_call_target="tpu_custom_call" | custom-call | tf_op jit(solution)/shard_map/pallas_call | solution.py:444
  126.6 1.9 %copy.20 = bf16[128,2048]{1,0:T(8,128)(2,1)} copy(bf16[128,2048]{1,0:T(8,128)(2,1)} %shard_map.118) | data formatting | bytes 1048576

commit v4 on v3

--- a/solution.py
+++ b/solution.py
@@ -126,37 +126,37 @@
     return (wide + combined).astype(jnp.bfloat16)
 
 
-def routing(ids, weights, experts, capacity):
-    rows, top_k = ids.shape
-    expert = lax.broadcasted_iota(jnp.int32, (rows, experts), 1)
-    total = jnp.sum(weights, axis=1, keepdims=True)
-    member = jnp.zeros((rows, experts), F32)
-    share = jnp.zeros((rows, experts), F32)
+def routing(meta, top_k, first, experts, capacity):
+    rows = meta.shape[1]
+    padded = max(experts, 16)
+    expert = lax.broadcasted_iota(jnp.int32, (padded, rows), 0) + first
+    expert = expert.astype(F32)
+    weights = meta[top_k : 2 * top_k]
+    total = jnp.sum(weights, axis=0, keepdims=True)
+    member = jnp.zeros((padded, rows), F32)
+    share = jnp.zeros((padded, rows), F32)
     for k in range(top_k):
-        hit = (ids[:, k : k + 1] == expert).astype(F32)
+        hit = jnp.where(meta[k : k + 1] == expert, 1.0, 0.0)
         member = member + hit
-        share = share + hit * (weights[:, k : k + 1] / total)
+        share = share + hit * (weights[k : k + 1] / total)
     before = (
         lax.broadcasted_iota(jnp.int32, (rows, rows), 0)
-        > lax.broadcasted_iota(jnp.int32, (rows, rows), 1)
+        < lax.broadcasted_iota(jnp.int32, (rows, rows), 1)
     ).astype(BF16)
-    rank = dot(before, member.astype(BF16))
-    rank = jnp.where(member > 0, rank, -1.0)
+    rank = jnp.where(member > 0, dot(member.astype(BF16), before), -1.0)
     slots = experts * capacity
     spread = (
-        lax.broadcasted_iota(jnp.int32, (experts, slots), 1) // capacity
-        == lax.broadcasted_iota(jnp.int32, (experts, slots), 0)
+        lax.broadcasted_iota(jnp.int32, (slots, padded), 0) // capacity
+        == lax.broadcasted_iota(jnp.int32, (slots, padded), 1)
     ).astype(BF16)
-    rank_slot = dot(rank.astype(BF16), spread)
-    place = lax.broadcasted_iota(jnp.int32, (rows, slots), 1) % capacity
-    taken = rank_slot == place.astype(F32)
+    place = lax.broadcasted_iota(jnp.int32, (slots, rows), 0) % capacity
+    one = jnp.where(dot(spread, rank.astype(BF16)) == place.astype(F32), 1.0, 0.0)
     high = share.astype(BF16)
     low = (share - high.astype(F32)).astype(BF16)
-    one = jnp.where(taken, 1.0, 0.0)
     return (
         one.astype(BF16),
-        (one * dot(high, spread)).astype(BF16),
-        (one * dot(low, spread)).astype(BF16),
+        (one * dot(spread, high)).astype(BF16),
+        (one * dot(spread, low)).astype(BF16),
     )
 
 
@@ -255,10 +255,13 @@
     halo, attended, halo_send, halo_recv,
     out_w, gate_w, up_w, down_w,
     pair_out, pair_in, far_out, far_in,
-    stream, normed, slots, share_hi, share_lo,
-    outbox, arrived, results, returned,
     load_sem, pair_send, pair_recv, far_send, far_recv,
-    go_send, go_recv, back_send, back_recv,
+    meta, meta_send, meta_recv,
+    stream, picks, share_hi, share_lo,
+    tokens, z_send, z_recv,
+    sel_out, rows_in, a_send, a_recv,
+    res_out, res_in, b_send, b_recv,
+    held, part_out, from_low, from_high, r_send, low_recv, high_recv,
 ):
     sp_count, tp_count, pieces, capacity = sizes
     experts = sp_count * tp_count
@@ -291,7 +294,19 @@
         return carry
 
     lax.fori_loop(1, experts, greet, 0)
+    top_k = ids.shape[0]
+    meta[z, 0:top_k] = ids[...].astype(F32)
+    meta[z, top_k : 2 * top_k] = weights[...]
     pl.semaphore_wait(barrier, experts - 1)
+
+    def meta_copy(to, at):
+        return pltpu.make_async_remote_copy(
+            meta.at[at], meta.at[at], meta_send.at[to], meta_recv.at[at],
+            device_id={"sp": to}, device_id_type=MESH,
+        )
+
+    for k in range(1, sp_count):
+        meta_copy((z + k) % sp_count, z).start()
     attend(sp_count, z, queries, kv, sink, halo, attended, halo_send, halo_recv)
     loads[0].wait()
 
@@ -321,7 +336,13 @@
             pair_copy(k, q).wait_recv()
             far_out[k, q] = (mine + pair_in[k, q].astype(F32)).astype(BF16)
             far_copy(k, q).start()
-    slots[...], share_hi[...], share_lo[...] = routing(ids[...], weights[...], experts, capacity)
+    for k in range(sp_count):
+        j = (z + k) % sp_count
+        if k:
+            meta_copy(z, j).wait_recv()
+        picks[j], share_hi[j], share_lo[j] = routing(
+            meta[j], top_k, z * tp_count, tp_count, capacity
+        )
     square = jnp.zeros((rows, 1), F32)
     for q in range(pieces):
         cols = slice(q * piece, (q + 1) * piece)
@@ -336,89 +357,187 @@
         value = value.astype(F32)
         square = square + jnp.sum(value * value, axis=1, keepdims=True)
     scale = lax.rsqrt(square / width + EPS)
+    last = sp_count - 1
+    above, below = jnp.minimum(z + 1, last), jnp.maximum(z - 1, 0)
+
+    def z_copy(j, q, to, lane):
+        return pltpu.make_async_remote_copy(
+            tokens.at[j, q], tokens.at[j, q], z_send.at[lane, j, q], z_recv.at[j, q],
+            device_id={"sp": to}, device_id_type=MESH,
+        )
+
+    def a_copy(j, q, to, at):
+        return pltpu.make_async_remote_copy(
+            sel_out.at[j, q, to], rows_in.at[j, q, at], a_send.at[j, q, to], a_recv.at[j, q, at],
+            device_id={"tp": to}, device_id_type=MESH,
+        )
+
+    def b_copy(j, q, to, at):
+        return pltpu.make_async_remote_copy(
+            res_out.at[j, q, to], res_in.at[j, q, at], b_send.at[j, q, to], b_recv.at[j, q, at],
+            device_id={"tp": to}, device_id_type=MESH,
+        )
+
+    def up_copy(j, q):
+        return pltpu.make_async_remote_copy(
+            part_out.at[j, q], from_low.at[j, q], r_send.at[j, q], low_recv.at[j, q],
+            device_id={"sp": above}, device_id_type=MESH,
+        )
+
+    def down_copy(j, q):
+        return pltpu.make_async_remote_copy(
+            part_out.at[j, q], from_high.at[j, q], r_send.at[j, q], high_recv.at[j, q],
+            device_id={"sp": below}, device_id_type=MESH,
+        )
+
     for q in range(pieces):
         cols = slice(q * piece, (q + 1) * piece)
-        normed[:, cols] = (stream[:, cols].astype(F32) * scale * gain[:, cols]).astype(BF16)
-
-    def go_copy(to, at):
-        return pltpu.make_async_remote_copy(
-            outbox.at[to], arrived.at[at], go_send.at[to], go_recv.at[at],
-            device_id=where(to), device_id_type=MESH,
-        )
-
-    def back_copy(to, at):
-        return pltpu.make_async_remote_copy(
-            results.at[to], returned.at[at], back_send.at[to], back_recv.at[at],
-            device_id=where(to), device_id_type=MESH,
-        )
-
-    picks = tp_count * capacity
-    for d in range(sp_count):
-        layer = range(d * tp_count, (d + 1) * tp_count)
-        chosen = dot(slots[:, d * picks : (d + 1) * picks], normed[...], ((0,), (0,))).astype(BF16)
-        for i, e in enumerate(layer):
-            outbox[e] = chosen[i * capacity : (i + 1) * capacity]
-
-            @pl.when(e != me)
+        tokens[z, q] = (stream[:, cols].astype(F32) * scale * gain[:, cols]).astype(BF16)
+
+        @pl.when(z < last)
+        def _():
+            z_copy(z, q, above, 0).start()
+
+        @pl.when(z > 0)
+        def _():
+            z_copy(z, q, below, 1).start()
+
+    sign = 1 - 2 * ((2 * z) // sp_count)
+    near = jnp.minimum(z, last - z)
+
+    def nth(step):
+        turn = (step + 1) // 2
+        turn = z + sign * (turn if step % 2 else -turn)
+        return jnp.where(2 * near >= step, turn, z + sign * (step - near))
+
+    slots = tp_count * capacity
+    peers = [(t + k) % tp_count for k in range(1, tp_count)]
+
+    def choose(step):
+        j = nth(step)
+        for q in range(pieces):
+            if step:
+                z_copy(j, q, z, 0).wait_recv()
+
+                @pl.when((j < z) & (z < last))
+                def _():
+                    z_copy(j, q, above, 0).start()
+
+                @pl.when((j > z) & (z > 0))
+                def _():
+                    z_copy(j, q, below, 0).start()
+
+            chosen = dot(picks[j], tokens[j, q]).astype(BF16)
+            sel_out[j, q] = chosen.reshape(tp_count, capacity, piece)
+            for i in peers:
+                a_copy(j, q, i, t).start()
+            rows_in[j, q, t] = sel_out[j, q, t]
+
+    def expert(step):
+        j = nth(step)
+        hidden = gate_w.shape[1]
+        gated = jnp.zeros((slots, hidden), F32)
+        raised = jnp.zeros((slots, hidden), F32)
+        for q in range(pieces):
+            for i in peers:
+                a_copy(j, q, t, i).wait_recv()
+            block = rows_in[j, q].reshape(slots, piece)
+            gated = gated + dot(block, gate_w[q * piece : (q + 1) * piece, :])
+            raised = raised + dot(block, up_w[q * piece : (q + 1) * piece, :])
+        active = (gated / (1.0 + jnp.exp(-gated)) * raised).astype(BF16)
+        for q in range(pieces):
+            done = dot(active, down_w[:, q * piece : (q + 1) * piece]).astype(BF16)
+            res_out[j, q] = done.reshape(tp_count, capacity, piece)
+            for i in peers:
+                b_copy(j, q, i, t).start()
+            res_in[j, q, t] = res_out[j, q, t]
+
+    def blend(step):
+        j = nth(step)
+        for q in range(pieces):
+            for i in peers:
+                b_copy(j, q, t, i).wait_recv()
+            block = res_in[j, q].reshape(slots, piece)
+            total = dot(share_hi[j], block, ((0,), (0,))) + dot(share_lo[j], block, ((0,), (0,)))
+            held[j, q] = total
+
+            @pl.when((j < z) & (z == last))
             def _():
-                go_copy(e, me).start()
-
-    arrived[me] = outbox[me]
-    for load in loads[1:]:
-        load.wait()
-
-    def expert(d, carry):
-        layer = (z + d) % sp_count
-        for i in range(tp_count):
-            e = layer * tp_count + i
-
-            @pl.when(e != me)
+                part_out[j, q] = total.astype(BF16)
+                down_copy(j, q).start()
+
+            @pl.when((j > z) & (z == 0))
             def _():
-                go_copy(me, e).wait_recv()
-
-        block = arrived[pl.ds(layer * tp_count, tp_count)].reshape(picks, width)
-        gated = dot(block, gate_w[...])
-        raised = dot(block, up_w[...])
-        hidden = (gated / (1.0 + jnp.exp(-gated)) * raised).astype(BF16)
-        done = dot(hidden, down_w[...]).astype(BF16)
-        results[pl.ds(layer * tp_count, tp_count)] = done.reshape(tp_count, capacity, width)
-        for i in range(tp_count):
-            e = layer * tp_count + i
-
-            @pl.when(e != me)
-            def _():
-                back_copy(e, me).start()
-
-        return carry
-
-    lax.fori_loop(0, sp_count, expert, 0)
-    returned[me] = results[me]
-
-    def collect(k, carry):
-        e = (me + k) % experts
-        back_copy(me, e).wait_recv()
-        return carry
-
-    lax.fori_loop(1, experts, collect, 0)
-    for q in range(pieces):
-        cols = slice(q * piece, (q + 1) * piece)
-        back = returned[:, :, cols].reshape(experts * capacity, piece)
-        mixed = dot(share_hi[...], back) + dot(share_lo[...], back)
-        out[:, cols] = (stream[:, cols].astype(F32) + mixed).astype(BF16)
-
+                part_out[j, q] = total.astype(BF16)
+                up_copy(j, q).start()
+
+    for step in range(sp_count):
+        choose(step)
+        if step:
+            blend(step - 1)
+        else:
+            for load in loads[1:]:
+                load.wait()
+        expert(step)
+    blend(last)
+
+    reach = [max(j, last - j) for j in range(sp_count)]
+    for far in sorted(set(reach)):
+        for q in range(pieces):
+            cols = slice(q * piece, (q + 1) * piece)
+            for j in [j for j in range(sp_count) if reach[j] == far]:
+
+                @pl.when((z >= j) & (z < last))
+                def _():
+                    down_copy(j, q).wait_recv()
+                    held[j, q] += from_high[j, q].astype(F32)
+
+                @pl.when((z <= j) & (z > 0))
+                def _():
+                    up_copy(j, q).wait_recv()
+                    held[j, q] += from_low[j, q].astype(F32)
+
+                @pl.when((z > j) & (z < last))
+                def _():
+                    part_out[j, q] = held[j, q].astype(BF16)
+                    down_copy(j, q).start()
+
+                @pl.when((z < j) & (z > 0))
+                def _():
+                    part_out[j, q] = held[j, q].astype(BF16)
+                    up_copy(j, q).start()
+
+                @pl.when(z == j)
+                def _():
+                    out[:, cols] = (stream[:, cols].astype(F32) + held[j, q]).astype(BF16)
+
+    for k in range(1, sp_count):
+        meta_copy((z + k) % sp_count, z).wait_send()
     for q in range(pieces):
         for k in range(chips):
             pair_copy(k, q).wait_send()
             if k:
                 far_copy(k, q).wait_send()
 
-    def flush(k, carry):
-        e = (me + k) % experts
-        go_copy(e, me).wait_send()
-        back_copy(e, me).wait_send()
-        return carry
-
-    lax.fori_loop(1, experts, flush, 0)
+        @pl.when(z < last)
+        def _():
+            z_copy(z, q, above, 0).wait_send()
+
+        @pl.when(z > 0)
+        def _():
+            z_copy(z, q, below, 1).wait_send()
+
+        for k in range(sp_count):
+            j = (z + k) % sp_count
+            for i in peers:
+                a_copy(j, q, i, t).wait_send()
+                b_copy(j, q, i, t).wait_send()
+            if k:
+                up_copy(j, q).wait_send()
+
+                @pl.when(((j < z) & (z < last)) | ((j > z) & (z > 0)))
+                def _():
+                    z_copy(j, q, above, 0).wait_send()
 
 
 def fused(
@@ -435,7 +554,8 @@
     pieces = 4
     chips = tp_count // 2
     part = (chips, pieces, rows, width // pieces)
-    box = (experts, capacity, width)
+    blocks = (sp_count, pieces, rows, width // pieces)
+    boxes = (sp_count, pieces, tp_count, capacity, width // pieces)
     seen, groups, size = key_heads.shape
     kv = jnp.stack([key_heads, value_heads], 2).reshape(seen, groups * 2 * size)
     vmem = pl.BlockSpec(memory_space=pltpu.VMEM)
@@ -459,30 +579,32 @@
             pltpu.VMEM(part, BF16),
             pltpu.VMEM(part, BF16),
             pltpu.VMEM(part, BF16),
-            pltpu.VMEM((rows, width), BF16),
-            pltpu.VMEM((rows, width), BF16),
-            pltpu.VMEM((rows, experts * capacity), BF16),
-            pltpu.VMEM((rows, experts * capacity), BF16),
-            pltpu.VMEM((rows, experts * capacity), BF16),
-            pltpu.VMEM(box, BF16),
-            pltpu.VMEM(box, BF16),
-            pltpu.VMEM(box, BF16),
-            pltpu.VMEM(box, BF16),
             dma((4,)),
             dma((chips, pieces)),
             dma((chips, pieces)),
             dma((chips, pieces)),
             dma((chips, pieces)),
-            dma((experts,)),
-            dma((experts,)),
-            dma((experts,)),
-            dma((experts,)),
+            pltpu.VMEM((sp_count, -(-2 * top_k // 8) * 8, rows), F32),
+            dma((sp_count,)),
+            dma((sp_count,)),
+            pltpu.VMEM((rows, width), BF16),
+            *[pltpu.VMEM((sp_count, tp_count * capacity, rows), BF16)] * 3,
+            pltpu.VMEM(blocks, BF16),
+            dma((2, sp_count, pieces)),
+            dma((sp_count, pieces)),
+            *[pltpu.VMEM(boxes, BF16)] * 2,
+            *[dma((sp_count, pieces, tp_count))] * 2,
+            *[pltpu.VMEM(boxes, BF16)] * 2,
+            *[dma((sp_count, pieces, tp_count))] * 2,
+            pltpu.VMEM(blocks, F32),
+            *[pltpu.VMEM(blocks, BF16)] * 3,
+            *[dma((sp_count, pieces))] * 3,
         ],
         compiler_params=pltpu.CompilerParams(
             collective_id=0, has_side_effects=True, vmem_limit_bytes=VMEM_BUDGET
         ),
     )(
-        queries, kv, sink_logit[None], out_weight, residual, norm_gain[None], expert_ids, route_weights,
+        queries, kv, sink_logit[None], out_weight, residual, norm_gain[None], expert_ids.T, route_weights.T,
         gate_weight, up_weight, down_weight,
     )
 

time: 129 us -> 162 us (1.26)
  the two profiles are of different devices: /device:TPU:31 before, /device:TPU:24 now
where the time goes in v4:
time: 162 us; the launch traced here: 161 us
  Pallas kernels  158 us (98%)
  local copies, waits for them, and re-layouts  2.64 us (2%)
    pallas_call x1, Pallas kernels, fused(): pl.pallas_call(functools.partial(tail_kernel, (sp_count, tp_count, pieces...  158 us

profile of v4, /device:TPU:24, one launch (start us, length us, event | category | flops | bytes accessed | tf_op | source)
XLA Modules:
  0.0 161.3 jit_solution(7410497475130688013)
XLA Ops:
  0.0 0.9 pad_maximum_fusion
  0.9 0.8 copy.14.kv
  1.6 157.8 %shard_map.118 = bf16[128,2048]{1,0:T(8,128)(2,1)} custom-call(bf16[512,512]{1,0:T(8,128)(2,1)} %queries.1, bf16[512,128]{1,0:T(8,128)(2,1)} %copy.14.kv, f32[1,8]{1,0:T(1,128)} %bitcast.13, bf16[512,2048]{1,0:T(8,128)(2,1)} %out_w_hbm.1, bf16[128,2048]{1,0:T(8,128)(2,1)} %residual.1, f32[1,2048]{1,0:T(1,128)} %bitcast.10, s32[2,128]{1,0:T(2,128)} %bitcast.11, ...), custom_call_target="tpu_custom_call" | custom-call | tf_op jit(solution)/shard_map/pallas_call | solution.py:564
  159.4 1.9 %copy.16 = bf16[128,2048]{1,0:T(8,128)(2,1)} copy(bf16[128,2048]{1,0:T(8,128)(2,1)} %shard_map.118) | data formatting | bytes 1048576

commit v5 on v3

--- a/solution.py
+++ b/solution.py
@@ -127,13 +127,16 @@
 
 
 def routing(ids, weights, experts, capacity):
-    rows, top_k = ids.shape
-    expert = lax.broadcasted_iota(jnp.int32, (rows, experts), 1)
+    top_k, rows = ids.shape
+    pad = jnp.zeros((-2 * top_k % 8, rows), F32)
+    facts = jnp.concatenate([ids.astype(F32), weights, pad], 0).T
+    ids, weights = facts[:, :top_k], facts[:, top_k : 2 * top_k]
+    expert = lax.broadcasted_iota(jnp.int32, (rows, experts), 1).astype(F32)
     total = jnp.sum(weights, axis=1, keepdims=True)
     member = jnp.zeros((rows, experts), F32)
     share = jnp.zeros((rows, experts), F32)
     for k in range(top_k):
-        hit = (ids[:, k : k + 1] == expert).astype(F32)
+        hit = jnp.where(ids[:, k : k + 1] == expert, 1.0, 0.0)
         member = member + hit
         share = share + hit * (weights[:, k : k + 1] / total)
     before = (
@@ -160,22 +163,13 @@
     )
 
 
-def attend(sp_count, z, queries, kv, sink, halo, attended, send, recv):
-    rows, lanes = kv.shape
-    window = halo.shape[0]
+def attend(z, token_rows, queries, sink, seen, attended, at):
+    window = WINDOW
+    rows, lanes = queries.shape[0], seen.shape[1]
     heads = sink.shape[1]
     size = queries.shape[1] // heads
     groups = lanes // (2 * size)
     share = heads // groups
-    copy = pltpu.make_async_remote_copy(
-        kv.at[pl.ds(rows - window, window)], halo, send, recv,
-        device_id={"sp": jnp.minimum(z + 1, sp_count - 1)}, device_id_type=MESH,
-    )
-
-    @pl.when(z < sp_count - 1)
-    def _():
-        copy.start()
-
     pairs = share // 2
     tall = pairs * window
     query = lax.broadcasted_iota(jnp.int32, (tall, 2 * window), 0) % window
@@ -184,13 +178,9 @@
     band = (distance >= 0) & (distance < window)
 
     def block(b):
-        allowed = band
-        if b == 0:
-            allowed = band & (z * rows - window + key >= 0)
-            span = jnp.concatenate([halo[...], kv[:window]], 0)
-        else:
-            span = kv[(b - 1) * window : (b + 1) * window]
-        here = slice(b * window, (b + 1) * window)
+        allowed = band & ((z * rows + b * window - window) + key >= 0)
+        span = seen[pl.ds(pl.multiple_of(b * window, window), 2 * window), :]
+        here = pl.ds(pl.multiple_of(b * window, window), window)
         for g in range(groups):
             keys = span[:, 2 * g * size : (2 * g + 1) * size]
             values = span[:, (2 * g + 1) * size : (2 * g + 2) * size]
@@ -230,29 +220,15 @@
                 first = (g * share + 2 * i) * size
                 attended[here, first : first + 2 * size] = both[i * window : (i + 1) * window]
 
-    for b in range(1, rows // window):
-        block(b)
-
-    @pl.when(z == 0)
-    def _():
-        halo[...] = jnp.zeros_like(halo)
-
-    @pl.when(z > 0)
-    def _():
-        copy.wait_recv()
-
-    block(0)
-
-    @pl.when(z < sp_count - 1)
-    def _():
-        copy.wait_send()
+    for b in range(token_rows // window):
+        block(at * (token_rows // window) + b)
 
 
 def tail_kernel(
     sizes,
     queries, kv, sink, out_w_hbm, residual, gain, ids, weights, gate_hbm, up_hbm, down_hbm,
     out,
-    halo, attended, halo_send, halo_recv,
+    seen, attended, halo_send, halo_recv,
     out_w, gate_w, up_w, down_w,
     pair_out, pair_in, far_out, far_in,
     stream, normed, slots, share_hi, share_lo,
@@ -292,7 +268,27 @@
 
     lax.fori_loop(1, experts, greet, 0)
     pl.semaphore_wait(barrier, experts - 1)
-    attend(sp_count, z, queries, kv, sink, halo, attended, halo_send, halo_recv)
+    reach = kv.shape[0]
+    halo_copy = pltpu.make_async_remote_copy(
+        kv.at[pl.ds(reach - WINDOW, WINDOW)], seen.at[pl.ds(0, WINDOW)], halo_send, halo_recv,
+        device_id={"sp": jnp.minimum(z + 1, sp_count - 1)}, device_id_type=MESH,
+    )
+
+    @pl.when(z < sp_count - 1)
+    def _():
+        halo_copy.start()
+
+    seen[WINDOW:, :] = kv[...]
+    slots[...], share_hi[...], share_lo[...] = routing(ids[...], weights[...], experts, capacity)
+
+    @pl.when(z == 0)
+    def _():
+        seen[:WINDOW, :] = jnp.zeros((WINDOW, kv.shape[1]), BF16)
+
+    @pl.when(z > 0)
+    def _():
+        halo_copy.wait_recv()
+
     loads[0].wait()
 
     def partial(chip, which, q):
@@ -312,16 +308,18 @@
         )
 
     order = list(range(1, chips)) + [0]
-    for q in range(pieces):
-        for k in order:
-            pair_out[k, q] = partial((x + k) % chips, other, q).astype(BF16)
+    for k in order:
+        chip = (x + k) % chips
+        attend(z, rows, queries, sink, seen, attended, chip * 2 + other)
+        for q in range(pieces):
+            pair_out[k, q] = partial(chip, other, q).astype(BF16)
             pair_copy(k, q).start()
-        for k in range(1, chips):
-            mine = partial((x + k) % chips, core, q)
+        attend(z, rows, queries, sink, seen, attended, chip * 2 + core)
+        for q in range(pieces if k else 0):
+            mine = partial(chip, core, q)
             pair_copy(k, q).wait_recv()
             far_out[k, q] = (mine + pair_in[k, q].astype(F32)).astype(BF16)
             far_copy(k, q).start()
-    slots[...], share_hi[...], share_lo[...] = routing(ids[...], weights[...], experts, capacity)
     square = jnp.zeros((rows, 1), F32)
     for q in range(pieces):
         cols = slice(q * piece, (q + 1) * piece)
@@ -406,6 +404,10 @@
         mixed = dot(share_hi[...], back) + dot(share_lo[...], back)
         out[:, cols] = (stream[:, cols].astype(F32) + mixed).astype(BF16)
 
+    @pl.when(z < sp_count - 1)
+    def _():
+        halo_copy.wait_send()
+
     for q in range(pieces):
         for k in range(chips):
             pair_copy(k, q).wait_send()
@@ -436,8 +438,8 @@
     chips = tp_count // 2
     part = (chips, pieces, rows, width // pieces)
     box = (experts, capacity, width)
-    seen, groups, size = key_heads.shape
-    kv = jnp.stack([key_heads, value_heads], 2).reshape(seen, groups * 2 * size)
+    reach, groups, size = key_heads.shape
+    kv = jnp.stack([key_heads, value_heads], 2).reshape(reach, groups * 2 * size)
     vmem = pl.BlockSpec(memory_space=pltpu.VMEM)
     hbm = pl.BlockSpec(memory_space=pl.ANY)
     dma = pltpu.SemaphoreType.DMA
@@ -447,7 +449,7 @@
         in_specs=[vmem, vmem, vmem, hbm, vmem, vmem, vmem, vmem, hbm, hbm, hbm],
         out_specs=vmem,
         scratch_shapes=[
-            pltpu.VMEM((WINDOW, kv.shape[1]), BF16),
+            pltpu.VMEM((WINDOW + kv.shape[0], kv.shape[1]), BF16),
             pltpu.VMEM(queries.shape, BF16),
             dma,
             dma,
@@ -482,7 +484,7 @@
             collective_id=0, has_side_effects=True, vmem_limit_bytes=VMEM_BUDGET
         ),
     )(
-        queries, kv, sink_logit[None], out_weight, residual, norm_gain[None], expert_ids, route_weights,
+        queries, kv, sink_logit[None], out_weight, residual, norm_gain[None], expert_ids.T, route_weights.T,
         gate_weight, up_weight, down_weight,
     )
 
@@ -490,7 +492,7 @@
 def on_device(queries, key_heads, value_heads, sink_logit, *rest):
     rows_dev = rest[1].shape[0]
     experts = lax.axis_size("sp") * lax.axis_size("tp")
-    fits = 2 * rest[3].shape[1] * rows_dev // experts % 16 == 0
+    fits = 2 * rest[3].shape[1] * rows_dev // experts % 16 == 0 and rows_dev % WINDOW == 0
     if fits:
         return fused(queries, key_heads, value_heads, sink_logit, *rest)
     return tail_plain(attention(queries, key_heads, value_heads, sink_logit), *rest)

time: 129 us -> 122 us (0.946)
  Pallas kernels: 122 us -> 118 us
  local copies, waits for them, and re-layouts: 5.45 us -> 2.64 us
    pallas_call x1, Pallas kernels: 122 us -> 118 us  [fused(): pl.pallas_call(functools.partial(tail_kernel, (sp_count, tp_count, pieces...]
    unnamed x3 -> x1, local copies, waits for them, and re-layouts: 4.69 us -> 1.88 us
where the time goes in v5:
time: 122 us
  Pallas kernels  118 us (97%)
  local copies, waits for them, and re-layouts  2.64 us (2%)
    pallas_call x1, Pallas kernels, fused(): pl.pallas_call(functools.partial(tail_kernel, (sp_count, tp_count, pieces...  118 us

profile of v5, /device:TPU:31, one launch (start us, length us, event | category | flops | bytes accessed | tf_op | source)
XLA Modules:
  0.0 121.7 jit_solution(12176368414457230718)
XLA Ops:
  0.0 0.9 pad_maximum_fusion
  0.9 0.8 copy.14.kv
  1.6 118.2 %shard_map.118 = bf16[128,2048]{1,0:T(8,128)(2,1)} custom-call(bf16[512,512]{1,0:T(8,128)(2,1)} %queries.1, bf16[512,128]{1,0:T(8,128)(2,1)} %copy.14.kv, f32[1,8]{1,0:T(1,128)} %bitcast.13, bf16[512,2048]{1,0:T(8,128)(2,1)} %out_w_hbm.1, bf16[128,2048]{1,0:T(8,128)(2,1)} %residual.1, f32[1,2048]{1,0:T(1,128)} %bitcast.10, s32[2,128]{1,0:T(2,128)} %bitcast.11, ...), custom_call_target="tpu_custom_call" | custom-call | tf_op jit(solution)/shard_map/pallas_call | solution.py:446
  119.8 1.9 %copy.16 = bf16[128,2048]{1,0:T(8,128)(2,1)} copy(bf16[128,2048]{1,0:T(8,128)(2,1)} %shard_map.118) | data formatting | bytes 1048576
